TPU v7x, 128 devices: a whole 4x4x4 slice. The times are simulated.
128 devices in a mesh: sp: 32 (over z, y, core), tp: 4 (over x).
Axes of the slice: x: 4, y: 4, z: 4, core: 2. Of those that a mesh axis runs over, the one named last changes fastest.
Arguments:
- tokens: bfloat16 [4, 2048, 1024], P(None, 'sp', 'tp'), may hold values from -6 to 6
- norm_gain: float32 [4, 1024], replicated, may hold values from 0.1 to 1.9
- val_weight: bfloat16 [4, 1024, 512], P(None, 'sp', 'tp'), may hold values from -0.1875 to 0.1875
- gate_weight: bfloat16 [4, 1024, 512], P(None, 'sp', 'tp'), may hold values from -0.1875 to 0.1875
- conv_taps: float32 [4, 31, 512], P(None, None, 'tp'), may hold values from -1 to 1
- conv_bias: float32 [4, 512], P(None, 'tp'), may hold values from -3 to 3
- ln_gain: float32 [4, 512], P(None, 'tp'), may hold values from 0.1 to 1.9
- ln_shift: float32 [4, 512], P(None, 'tp'), may hold values from -3 to 3
- out_weight: bfloat16 [4, 512, 1024], P(None, 'tp', 'sp'), may hold values from -0.25 to 0.25
Outputs:
- stream: bfloat16 [4, 2048, 1024], P(None, 'sp', 'tp')
All inputs are finite; a program needn't handle non-finite values.
Results may differ from a plain program's by a relative error of at most 0.02.
Values may be sent and summed in bfloat16 or wider, within the bound.
A program may use at most 64 MiB of HBM per device.

v0:
```python
from functools import partial

import jax
import jax.numpy as jnp
from jax import lax
from jax.sharding import PartitionSpec as P

LAYERS = 4


epsilon = 1e-06


def over_all(shard, axis, dim, absorb, state):
    everything = jax.tree.map(lambda a: lax.all_gather(a, axis, axis=dim, tiled=True), shard)
    return absorb(state, everything, jnp.int32(0))


def with_halo(shard, sides, width, wrap):
    for axis, dim in sides:
        size, length = lax.axis_size(axis), shard.shape[dim]
        up = [(i, (i + 1) % size) for i in range(size if wrap else size - 1)]
        down = [(j, i) for i, j in up]
        last = lax.slice_in_dim(shard, length - width, length, axis=dim)
        initial = lax.slice_in_dim(shard, 0, width, axis=dim)
        before = lax.ppermute(last, axis, up)
        after = lax.ppermute(initial, axis, down)
        shard = jnp.concatenate([before, shard, after], axis=dim)
    return shard


def together(arrays, axis):
    ends = [0]
    for a in arrays:
        ends.append(ends[-1] + a.size)
    subtotal = lax.psum(jnp.concatenate([a.ravel() for a in arrays]), axis)
    return tuple(subtotal[b:e].reshape(a.shape) for a, b, e in zip(arrays, ends, ends[1:]))


def on_whole(shard, axis, dim, work):
    return work(lax.all_gather(shard, axis, axis=dim, tiled=True), jnp.int32(0))


def depthwise(padded, tap_weights, length):
    running = padded[:, 0:length] * tap_weights[0]
    for tap_idx in range(1, tap_weights.shape[0]):
        running = running + padded[:, tap_idx : tap_idx + length] * tap_weights[tap_idx]
    return running


def add_rows(left_rows, running, shard_piece, offset):
    columns = lax.dynamic_slice_in_dim(left_rows, offset, shard_piece.shape[0], 1)
    return running + jnp.dot(columns, shard_piece, preferred_element_type=jnp.float32)


def add_both(left_rows, totals, pieces, offset):
    return (
        add_rows(left_rows, totals[0], pieces[0], offset),
        add_rows(left_rows, totals[1], pieces[1], offset),
    )


def project_rows(left_rows, shard_piece, offset):
    return jnp.dot(left_rows, shard_piece, preferred_element_type=jnp.float32)


def shards(
    tokens, norm_gain, val_weight, gate_weight, conv_taps, conv_bias, ln_gain, ln_shift, out_weight
):
    stream = tokens
    num_seqs = tokens.shape[0]
    local_len = tokens.shape[1]
    chan_width = val_weight.shape[2]
    all_channels = chan_width * lax.axis_size("tp")
    half_width = conv_taps.shape[1] // 2
    for layer_idx in range(LAYERS):
        gathered = lax.all_gather(stream, "tp", axis=2, tiled=True)
        widened = gathered.astype(jnp.float32)
        scaled = widened * lax.rsqrt(jnp.mean(widened * widened, axis=-1, keepdims=True) + epsilon)
        normed = (scaled * norm_gain[layer_idx]).astype(jnp.bfloat16)
        tok_rows = normed.reshape(-1, normed.shape[2])
        zeroed = jnp.zeros((tok_rows.shape[0], chan_width), jnp.float32)
        values, gates = over_all(
            (val_weight[layer_idx], gate_weight[layer_idx]),
            "sp",
            0,
            partial(add_both, tok_rows),
            (zeroed, zeroed),
        )
        gated = (
            (values * jax.nn.sigmoid(gates))
            .astype(jnp.bfloat16)
            .reshape(num_seqs, local_len, chan_width)
        )
        padded = with_halo(gated, (("sp", 1),), half_width, False)
        convolved = (
            depthwise(padded.astype(jnp.float32), conv_taps[layer_idx], local_len)
            + conv_bias[layer_idx]
        )
        first_sum, second_sum = together(
            (jnp.sum(convolved, axis=-1), jnp.sum(convolved * convolved, axis=-1)), "tp"
        )
        mean_val = (first_sum / all_channels)[..., None]
        spread = (second_sum / all_channels)[..., None] - mean_val * mean_val
        centered = convolved - mean_val
        normalized = (
            centered * lax.rsqrt(spread + epsilon) * ln_gain[layer_idx] + ln_shift[layer_idx]
        )
        activated = jax.nn.silu(normalized).astype(jnp.bfloat16).reshape(-1, chan_width)
        partial_terms = on_whole(out_weight[layer_idx], "sp", 1, partial(project_rows, activated))
        full_width = partial_terms.shape[1]
        summed = lax.psum_scatter(
            partial_terms.reshape(num_seqs, local_len, full_width).astype(jnp.bfloat16),
            "tp",
            scatter_dimension=2,
            tiled=True,
        ).astype(jnp.float32)
        stream = (stream.astype(jnp.float32) + summed).astype(jnp.bfloat16)
    return stream


def solution(mesh):
    return jax.shard_map(
        shards,
        mesh=mesh,
        in_specs=(
            P(None, "sp", "tp"),
            P(),
            P(None, "sp", "tp"),
            P(None, "sp", "tp"),
            P(None, None, "tp"),
            P(None, "tp"),
            P(None, "tp"),
            P(None, "tp"),
            P(None, "tp", "sp"),
        ),
        out_specs=P(None, "sp", "tp"),
        check_vma=False,
    )
```

profile of v0, /device:TPU:1, one launch (start us, length us, event | category | flops | bytes accessed | tf_op | source)
XLA Modules:
  0.0 451.9 jit_solution(18299880186058381866)
XLA Ops:
  6.5 0.9 fusion.211
  7.4 12.5 %all_gather.48 = bf16[4,64,1024]{2,1,0:T(8,128)(2,1)S(1)} all-gather(bf16[4,64,256]{2,1,0:T(8,128)(2,1)} %param.9), channel_id=1, replica_groups=mesh['sp'=32,'tp'=4] {'tp'}, dimensions={2}, use_global_device_ids=true | all-gather | bytes 655360 | tf_op jit(solution)/shard_map/all_gather | solution.py:77
  19.9 0.2 fusion.20
  20.1 0.6 copy-done.2
  20.7 28.5 %all-gather = bf16[1,1024,128]{2,1,0:T(8,128)(2,1)S(1)} all-gather(bf16[1,32,128]{2,1,0:T(8,128)(2,1)S(1)} %get-tuple-element.155), channel_id=2, replica_groups=mesh['sp'=32,'tp'=4] {'sp'}, dimensions={1}, use_global_device_ids=true | all-gather | bytes 270336 | tf_op jit(solution)/shard_map/all_gather | solution.py:15
  49.2 24.1 %all-gather.1 = bf16[1,1024,128]{2,1,0:T(8,128)(2,1)S(1)} all-gather(bf16[1,32,128]{2,1,0:T(8,128)(2,1)S(1)} %get-tuple-element.151), channel_id=3, replica_groups=mesh['sp'=32,'tp'=4] {'sp'}, dimensions={1}, use_global_device_ids=true | all-gather | bytes 270336 | tf_op jit(solution)/shard_map/all_gather | solution.py:15
  73.3 0.2 fusion.22
  73.5 0.3 fusion.46
  73.8 0.3 fusion.16
  74.1 1.9 collective-permute-start
  76.0 2.4 collective-permute-start.1
  78.5 0.7 copy-done.5
  79.2 0.7 copy-done.6
  79.9 25.7 %all-gather.2 = bf16[1,128,1024]{1,2,0:T(8,128)(2,1)S(1)} all-gather(bf16[1,128,32]{1,2,0:T(8,128)(2,1)S(1)} %get-tuple-element.157), channel_id=4, replica_groups=mesh['sp'=32,'tp'=4] {'sp'}, dimensions={2}, use_global_device_ids=true | all-gather | bytes 270336 | tf_op jit(solution)/shard_map/all_gather | solution.py:41
  105.6 0.6 fusion.199
  106.4 8.7 %psum.28 = f32[512]{0:T(512)S(1)} all-reduce(f32[512]{0:T(512)S(1)} %pad_maximum_fusion), channel_id=1, replica_groups=mesh['sp'=32,'tp'=4] {'tp'}, use_global_device_ids=true, to_apply=%region_3.0 | all-reduce | flops 512 | bytes 4096 | tf_op jit(solution)/shard_map/psum | solution.py:36
  115.1 0.1 div.80
  115.2 1.2 convolution_convert_fusion.3
  116.5 24.9 %all-gather.3 = bf16[1,1024,128]{2,1,0:T(8,128)(2,1)S(1)} all-gather(bf16[1,32,128]{2,1,0:T(8,128)(2,1)S(1)} %get-tuple-element.154), channel_id=5, replica_groups=mesh['sp'=32,'tp'=4] {'sp'}, dimensions={1}, use_global_device_ids=true | all-gather | bytes 270336 | tf_op jit(solution)/shard_map/all_gather | solution.py:15
  141.4 23.7 %all-gather.4 = bf16[1,1024,128]{2,1,0:T(8,128)(2,1)S(1)} all-gather(bf16[1,32,128]{2,1,0:T(8,128)(2,1)S(1)} %get-tuple-element.150), channel_id=6, replica_groups=mesh['sp'=32,'tp'=4] {'sp'}, dimensions={1}, use_global_device_ids=true | all-gather | bytes 270336 | tf_op jit(solution)/shard_map/all_gather | solution.py:15
  165.1 0.9 add_convert_fusion.3
  166.1 10.3 %all_gather.52 = bf16[4,64,1024]{2,1,0:T(8,128)(2,1)S(1)} all-gather(bf16[4,64,256]{2,1,0:T(8,128)(2,1)S(1)} %add_convert_fusion.3), channel_id=1, replica_groups=mesh['sp'=32,'tp'=4] {'tp'}, dimensions={2}, use_global_device_ids=true | all-gather | bytes 655360 | tf_op jit(solution)/shard_map/all_gather | solution.py:77
  176.4 0.2 fusion.23
  176.6 0.2 fusion.25
  176.8 0.3 fusion.43
  177.1 0.3 fusion.17
  177.4 5.0 %collective-permute-start.2 = (bf16[4,15,128]{2,1,0:T(8,128)(2,1)S(1)}, bf16[4,15,128]{2,1,0:T(8,128)(2,1)S(1)}, u32[]{:S(2)}, u32[]{:S(2)}) collective-permute-start(bf16[4,15,128]{2,1,0:T(8,128)(2,1)S(1)} %get-tuple-element.21), channel_id=1, source_target_pairs={{0,4},{4,8},{8,12},{12,16},{16,20},{20,24},{24,28},{28,32},{32,36}... | collective-permute-start | bytes 46088 | tf_op jit(solution)/shard_map/ppermute | solution.py:26
  182.4 1.9 collective-permute-start.3
  184.3 27.1 %all-gather.5 = bf16[1,128,1024]{1,2,0:T(8,128)(2,1)S(1)} all-gather(bf16[1,128,32]{1,2,0:T(8,128)(2,1)S(1)} %get-tuple-element.158), channel_id=7, replica_groups=mesh['sp'=32,'tp'=4] {'sp'}, dimensions={2}, use_global_device_ids=true | all-gather | bytes 270336 | tf_op jit(solution)/shard_map/all_gather | solution.py:41
  211.5 0.6 fusion.198
  212.2 6.0 %psum.29 = f32[512]{0:T(512)S(1)} all-reduce(f32[512]{0:T(512)S(1)} %pad_maximum_fusion.1), channel_id=1, replica_groups=mesh['sp'=32,'tp'=4] {'tp'}, use_global_device_ids=true, to_apply=%region_8.9 | all-reduce | flops 512 | bytes 4096 | tf_op jit(solution)/shard_map/psum | solution.py:36
  218.2 0.1 div.87
  218.4 1.2 convolution_convert_fusion.2
  219.6 24.1 %all-gather.6 = bf16[1,1024,128]{2,1,0:T(8,128)(2,1)S(1)} all-gather(bf16[1,32,128]{2,1,0:T(8,128)(2,1)S(1)} %get-tuple-element.156), channel_id=8, replica_groups=mesh['sp'=32,'tp'=4] {'sp'}, dimensions={1}, use_global_device_ids=true | all-gather | bytes 270336 | tf_op jit(solution)/shard_map/all_gather | solution.py:15
  243.7 24.1 %all-gather.7 = bf16[1,1024,128]{2,1,0:T(8,128)(2,1)S(1)} all-gather(bf16[1,32,128]{2,1,0:T(8,128)(2,1)S(1)} %get-tuple-element.152), channel_id=9, replica_groups=mesh['sp'=32,'tp'=4] {'sp'}, dimensions={1}, use_global_device_ids=true | all-gather | bytes 270336 | tf_op jit(solution)/shard_map/all_gather | solution.py:15
  267.9 0.9 add_convert_fusion.2
  268.8 10.3 %all_gather.56 = bf16[4,64,1024]{2,1,0:T(8,128)(2,1)S(1)} all-gather(bf16[4,64,256]{2,1,0:T(8,128)(2,1)S(1)} %add_convert_fusion.2), channel_id=1, replica_groups=mesh['sp'=32,'tp'=4] {'tp'}, dimensions={2}, use_global_device_ids=true | all-gather | bytes 655360 | tf_op jit(solution)/shard_map/all_gather | solution.py:77
  279.1 0.2 fusion.26
  279.3 0.2 fusion.28
  279.5 0.3 fusion.40
  279.8 0.3 fusion.18
  280.1 3.8 collective-permute-start.4
  283.9 2.2 collective-permute-start.5
  286.1 26.7 %all-gather.8 = bf16[1,128,1024]{1,2,0:T(8,128)(2,1)S(1)} all-gather(bf16[1,128,32]{1,2,0:T(8,128)(2,1)S(1)} %get-tuple-element.160), channel_id=10, replica_groups=mesh['sp'=32,'tp'=4] {'sp'}, dimensions={2}, use_global_device_ids=true | all-gather | bytes 270336 | tf_op jit(solution)/shard_map/all_gather | solution.py:41
  312.8 0.6 fusion.197
  313.5 7.9 %psum.30 = f32[512]{0:T(512)S(1)} all-reduce(f32[512]{0:T(512)S(1)} %pad_maximum_fusion.2), channel_id=1, replica_groups=mesh['sp'=32,'tp'=4] {'tp'}, use_global_device_ids=true, to_apply=%region_13.14 | all-reduce | flops 512 | bytes 4096 | tf_op jit(solution)/shard_map/psum | solution.py:36
  321.6 1.2 convolution_convert_fusion.1
  322.9 24.9 %all-gather.9 = bf16[1,1024,128]{2,1,0:T(8,128)(2,1)S(1)} all-gather(bf16[1,32,128]{2,1,0:T(8,128)(2,1)S(1)} %get-tuple-element.153), channel_id=11, replica_groups=mesh['sp'=32,'tp'=4] {'sp'}, dimensions={1}, use_global_device_ids=true | all-gather | bytes 270336 | tf_op jit(solution)/shard_map/all_gather | solution.py:15
  347.8 23.8 %all-gather.10 = bf16[1,1024,128]{2,1,0:T(8,128)(2,1)S(1)} all-gather(bf16[1,32,128]{2,1,0:T(8,128)(2,1)S(1)} %get-tuple-element.149), channel_id=12, replica_groups=mesh['sp'=32,'tp'=4] {'sp'}, dimensions={1}, use_global_device_ids=true | all-gather | bytes 270336 | tf_op jit(solution)/shard_map/all_gather | solution.py:15
  371.6 0.9 add_convert_fusion.1
  372.5 10.3 %all_gather.60 = bf16[4,64,1024]{2,1,0:T(8,128)(2,1)S(1)} all-gather(bf16[4,64,256]{2,1,0:T(8,128)(2,1)S(1)} %add_convert_fusion.1), channel_id=1, replica_groups=mesh['sp'=32,'tp'=4] {'tp'}, dimensions={2}, use_global_device_ids=true | all-gather | bytes 655360 | tf_op jit(solution)/shard_map/all_gather | solution.py:77
  382.8 0.2 fusion.29
  383.0 0.2 fusion.31
  383.2 0.3 fusion.37
  383.5 0.3 fusion.19
  383.8 5.0 %collective-permute-start.6 = (bf16[4,15,128]{2,1,0:T(8,128)(2,1)S(1)}, bf16[4,15,128]{2,1,0:T(8,128)(2,1)S(1)}, u32[]{:S(2)}, u32[]{:S(2)}) collective-permute-start(bf16[4,15,128]{2,1,0:T(8,128)(2,1)S(1)} %get-tuple-element.17), channel_id=1, source_target_pairs={{0,4},{4,8},{8,12},{12,16},{16,20},{20,24},{24,28},{28,32},{32,36}... | collective-permute-start | bytes 46088 | tf_op jit(solution)/shard_map/ppermute | solution.py:26
  388.8 1.9 collective-permute-start.7
  390.8 26.9 %all-gather.11 = bf16[1,128,1024]{1,2,0:T(8,128)(2,1)S(1)} all-gather(bf16[1,128,32]{1,2,0:T(8,128)(2,1)S(1)} %get-tuple-element.159), channel_id=13, replica_groups=mesh['sp'=32,'tp'=4] {'sp'}, dimensions={2}, use_global_device_ids=true | all-gather | bytes 270336 | tf_op jit(solution)/shard_map/all_gather | solution.py:41
  417.7 0.6 fusion.196
  418.5 6.0 %psum.31 = f32[512]{0:T(512)S(1)} all-reduce(f32[512]{0:T(512)S(1)} %pad_maximum_fusion.3), channel_id=1, replica_groups=mesh['sp'=32,'tp'=4] {'tp'}, use_global_device_ids=true, to_apply=%region_18.19 | all-reduce | flops 512 | bytes 4096 | tf_op jit(solution)/shard_map/psum | solution.py:36
  424.5 0.1 div.101
  424.6 1.2 convolution_convert_fusion
  425.8 18.0 %reduce-scatter.11.cloned.1.call-done = bf16[4,64,256]{2,1,0:T(8,128)(2,1)} async-done(((bf16[4,64,1024]{2,1,0:T(8,128)(2,1)}), bf16[4,64,256]{2,1,0:T(8,128)(2,1)}) %reduce-scatter.11.cloned.1.call-update) | async-done | bytes 131088 | tf_op jit(solution)/shard_map/reduce_scatter | solution.py:112
  443.8 1.6 add_convert_fusion
  (81 shorter events, 1.8 us)
Async XLA Ops:
  6.5 158.6 %reduce-scatter.5.cloned.1.call-start = ((), (), s32[]{:S(2)}) async-start(), calls=%async_computation.4 | async-start | bytes 655360 | tf_op jit(solution)/shard_map/reduce_scatter | solution.py:112
  19.9 0.8 copy-start.2
  20.7 28.5 %copy-start.3 = (bf16[4,32,128]{2,1,0:T(8,128)(2,1)S(1)}, bf16[4,32,128]{2,1,0:T(8,128)(2,1)}, u32[]{:S(2)}) copy-start(bf16[4,32,128]{2,1,0:T(8,128)(2,1)} %param.12) | copy-start | bytes 98308
  74.1 4.4 copy-start.1
  74.1 5.1 %copy-start.4 = (bf16[4,128,32]{1,2,0:T(8,128)(2,1)S(1)}, bf16[4,128,32]{1,2,0:T(8,128)(2,1)}, u32[]{:S(2)}) copy-start(bf16[4,128,32]{1,2,0:T(8,128)(2,1)} %param.17) | copy-start | bytes 98308
  74.1 31.5 %collective-permute-start = (bf16[4,15,128]{2,1,0:T(8,128)(2,1)S(1)}, bf16[4,15,128]{2,1,0:T(8,128)(2,1)S(1)}, u32[]{:S(2)}, u32[]{:S(2)}) collective-permute-start(bf16[4,15,128]{2,1,0:T(8,128)(2,1)S(1)} %get-tuple-element.23), channel_id=1, source_target_pairs={{0,4},{4,8},{8,12},{12,16},{16,20},{20,24},{24,28},{28,32},{32,36}... | collective-permute-start | bytes 46088 | tf_op jit(solution)/shard_map/ppermute | solution.py:26
  76.0 29.6 %collective-permute-start.1 = (bf16[4,15,128]{2,1,0:T(8,128)(2,1)S(1)}, bf16[4,15,128]{2,1,0:T(8,128)(2,1)S(1)}, u32[]{:S(2)}, u32[]{:S(2)}) collective-permute-start(bf16[4,15,128]{2,1,0:T(8,128)(2,1)S(1)} %get-tuple-element.24), channel_id=1, source_target_pairs={{4,0},{8,4},{12,8},{16,12},{20,16},{24,20},{28,24},{32,28},{36,32}... | collective-permute-start | bytes 46088 | tf_op jit(solution)/shard_map/ppermute | solution.py:27
  78.5 0.7 copy-start.5
  79.2 0.7 copy-start.6
  79.2 0.7 copy-start.7
  116.4 151.4 %reduce-scatter.7.cloned.1.call-start = ((), (), s32[]{:S(2)}) async-start(), calls=%async_computation.5 | async-start | bytes 655360 | tf_op jit(solution)/shard_map/reduce_scatter | solution.py:112
  141.4 23.7 %copy-start = (bf16[4,64,256]{2,1,0:T(8,128)(2,1)S(1)}, bf16[4,64,256]{2,1,0:T(8,128)(2,1)}, u32[]{:S(2)}) copy-start(bf16[4,64,256]{2,1,0:T(8,128)(2,1)} %param.9) | copy-start | bytes 393220
  177.4 34.0 %collective-permute-start.2 = (bf16[4,15,128]{2,1,0:T(8,128)(2,1)S(1)}, bf16[4,15,128]{2,1,0:T(8,128)(2,1)S(1)}, u32[]{:S(2)}, u32[]{:S(2)}) collective-permute-start(bf16[4,15,128]{2,1,0:T(8,128)(2,1)S(1)} %get-tuple-element.21), channel_id=1, source_target_pairs={{0,4},{4,8},{8,12},{12,16},{16,20},{20,24},{24,28},{28,32},{32,36}... | collective-permute-start | bytes 46088 | tf_op jit(solution)/shard_map/ppermute | solution.py:26
  182.4 29.0 %collective-permute-start.3 = (bf16[4,15,128]{2,1,0:T(8,128)(2,1)S(1)}, bf16[4,15,128]{2,1,0:T(8,128)(2,1)S(1)}, u32[]{:S(2)}, u32[]{:S(2)}) collective-permute-start(bf16[4,15,128]{2,1,0:T(8,128)(2,1)S(1)} %get-tuple-element.22), channel_id=1, source_target_pairs={{4,0},{8,4},{12,8},{16,12},{20,16},{24,20},{28,24},{32,28},{36,32}... | collective-permute-start | bytes 46088 | tf_op jit(solution)/shard_map/ppermute | solution.py:27
  219.5 152.0 %reduce-scatter.9.cloned.1.call-start = ((), (), s32[]{:S(2)}) async-start(), calls=%async_computation.6 | async-start | bytes 655360 | tf_op jit(solution)/shard_map/reduce_scatter | solution.py:112
  280.1 32.6 %collective-permute-start.4 = (bf16[4,15,128]{2,1,0:T(8,128)(2,1)S(1)}, bf16[4,15,128]{2,1,0:T(8,128)(2,1)S(1)}, u32[]{:S(2)}, u32[]{:S(2)}) collective-permute-start(bf16[4,15,128]{2,1,0:T(8,128)(2,1)S(1)} %get-tuple-element.19), channel_id=1, source_target_pairs={{0,4},{4,8},{8,12},{12,16},{16,20},{20,24},{24,28},{28,32},{32,36}... | collective-permute-start | bytes 46088 | tf_op jit(solution)/shard_map/ppermute | solution.py:26
  283.9 28.9 %collective-permute-start.5 = (bf16[4,15,128]{2,1,0:T(8,128)(2,1)S(1)}, bf16[4,15,128]{2,1,0:T(8,128)(2,1)S(1)}, u32[]{:S(2)}, u32[]{:S(2)}) collective-permute-start(bf16[4,15,128]{2,1,0:T(8,128)(2,1)S(1)} %get-tuple-element.20), channel_id=1, source_target_pairs={{4,0},{8,4},{12,8},{16,12},{20,16},{24,20},{28,24},{32,28},{36,32}... | collective-permute-start | bytes 46088 | tf_op jit(solution)/shard_map/ppermute | solution.py:27
  322.8 121.0 %reduce-scatter.11.cloned.1.call-start = ((), (), s32[]{:S(2)}) async-start(), calls=%async_computation.7 | async-start | bytes 655360 | tf_op jit(solution)/shard_map/reduce_scatter | solution.py:112
  383.8 33.9 %collective-permute-start.6 = (bf16[4,15,128]{2,1,0:T(8,128)(2,1)S(1)}, bf16[4,15,128]{2,1,0:T(8,128)(2,1)S(1)}, u32[]{:S(2)}, u32[]{:S(2)}) collective-permute-start(bf16[4,15,128]{2,1,0:T(8,128)(2,1)S(1)} %get-tuple-element.17), channel_id=1, source_target_pairs={{0,4},{4,8},{8,12},{12,16},{16,20},{20,24},{24,28},{28,32},{32,36}... | collective-permute-start | bytes 46088 | tf_op jit(solution)/shard_map/ppermute | solution.py:26
  388.8 28.9 %collective-permute-start.7 = (bf16[4,15,128]{2,1,0:T(8,128)(2,1)S(1)}, bf16[4,15,128]{2,1,0:T(8,128)(2,1)S(1)}, u32[]{:S(2)}, u32[]{:S(2)}) collective-permute-start(bf16[4,15,128]{2,1,0:T(8,128)(2,1)S(1)} %get-tuple-element.18), channel_id=1, source_target_pairs={{4,0},{8,4},{12,8},{16,12},{20,16},{24,20},{28,24},{32,28},{36,32}... | collective-permute-start | bytes 46088 | tf_op jit(solution)/shard_map/ppermute | solution.py:27
Sparse Core Ops, SparseCore 0:
  116.6 17.4 reduce-scatter.4
  219.7 17.8 reduce-scatter.6
  322.9 17.4 reduce-scatter.8
  425.9 17.8 reduce-scatter.10
where the time goes:
time: 455 us; the launch traced here: 452 us
  blocking collectives  376 us (83%)
  starting transfers between devices  24.3 us (5%)
  waiting for transfers between devices  18.1 us (4%)
  between operations  13.5 us (3%)
  other arithmetic  8.4 us (2%)
  matrix products  7 us (2%)
    all_gather x8, blocking collectives, over_all(): lax.all_gather(a, axis, axis=dim, tiled=True)  198 us
    all_gather x4, blocking collectives, on_whole(): return work(lax.all_gather(shard, axis, axis=dim, tiled=True), jnp.int32(0))  106 us
    all_gather x4, blocking collectives, shards(): gathered = lax.all_gather(stream, 'tp', axis=2, tiled=True)  43.3 us
    psum x4, blocking collectives, together(): subtotal = lax.psum(jnp.concatenate([a.ravel() for a in arrays]), axis)  28.6 us
    reduce_scatter x4, waiting for transfers between devices, shards(): lax.psum_scatter(partial_terms.reshape(num_seqs, local_len, full_width).a...  18 us
    ppermute x4, starting transfers between devices, with_halo(): before = lax.ppermute(last, axis, up)  15.7 us
  transfers between devices with their start and end apart: 12, of which 1 were waited for; matrix products, arithmetic and copies ran while one was open for 0% of the time, Pallas kernels for 0%

commit v1 on v0

v1 whole, which is shorter than its diff:
```python
import jax
import jax.numpy as jnp
from jax import lax
from jax.experimental import pallas as pl
from jax.experimental.pallas import tpu as pltpu
from jax.sharding import PartitionSpec as P

MESH = pl.DeviceIdType.MESH
LAYERS = 4
TAPS = 31
HALF = 15
EPS = 1e-6
LOCAL = 64
ROWS = 192
STEP = 16
ORDERS = (("x", "y", "z"), ("y", "z", "x"), ("z", "x", "y"))
F32 = jnp.float32
BF16 = jnp.bfloat16


def kernel(
    tokens, norm_gain, val_w, gate_w, out_w, taps, bias, ln_gain, ln_shift, out,
    w, x_buf, g_buf, c_buf, nb, tap_all, vec_all,
    load_sem, send_sem, first_sem, rest_sem, sib_send, sib_recv, tok_sem, par_sem, end_sem,
):
    sp = lax.axis_index("sp")
    x = lax.axis_index("tp")
    z = sp // 8
    y = (sp // 2) % 4
    c = sp % 2
    at = {"x": x, "y": y, "z": z}
    sibling = (sp + 1 - 2 * c, x)

    def near(axis, step):
        if axis == "x":
            return (sp, (x + step) % 4)
        if axis == "y":
            return (z * 8 + ((y + step) % 4) * 2 + c, x)
        return (((z + step) % 4) * 8 + y * 2 + c, x)

    before = ((sp + 31) % 32, x)
    after = ((sp + 1) % 32, x)
    outer = ((sp + 32 + (2 * c - 1)) % 32, x)

    loads = []
    for k, array in enumerate((val_w, gate_w, out_w)):
        d1, d2, d3 = ORDERS[k]
        loads.append(
            pltpu.make_async_copy(
                array, w.at[:, k, c, at[d3], at[d2], at[d1]], load_sem.at[k]
            )
        )
    loads.append(pltpu.make_async_copy(taps, tap_all.at[x], load_sem.at[3]))
    for j, array in enumerate((bias, ln_gain, ln_shift)):
        loads.append(pltpu.make_async_copy(array, vec_all.at[x, j], load_sem.at[4 + j]))
    own_cols = pl.ds(pl.multiple_of(x * 256, 256), 256)
    loads.append(
        pltpu.make_async_copy(
            tokens.at[x], x_buf.at[pl.ds(LOCAL, LOCAL), own_cols], load_sem.at[7]
        )
    )
    for load in loads:
        load.start()

    barrier = pltpu.get_barrier_semaphore()
    peers = [near(a, s) for a in "xyz" for s in (1, 3)] + [near("x", 2), sibling, outer]
    for peer in peers:
        pl.semaphore_signal(barrier, inc=1, device_id=peer, device_id_type=MESH)
    pl.semaphore_wait(barrier, len(peers))

    def send(ref, dst, peer, s_sem, r_sem):
        pltpu.make_async_remote_copy(
            src_ref=ref, dst_ref=dst, send_sem=s_sem, recv_sem=r_sem,
            device_id=peer, device_id_type=MESH,
        ).start()

    def wait_bytes(ref, sem):
        pltpu.make_async_copy(ref, ref, sem).wait()

    def block(k, phase, layer, index, half):
        d1, d2, d3 = ORDERS[k]
        if phase == 2:
            part = slice(None) if half is None else pl.ds(2 * half, 2)
            return w.at[layer, k, c, index, part]
        part = slice(None) if half is None else pl.ds(2 * half, 2)
        if phase == 0:
            return w.at[part, k, c, at[d3], at[d2], index]
        return w.at[part, k, c, at[d3], index]

    def sems(k, phase, layer):
        return (k, phase if phase < 2 else 2 + layer)

    def own_half(k, phase, layer, which):
        axis = ORDERS[k][phase]
        q, s = sems(k, phase, layer)
        for way, half in ((0, which), (1, 1 - which)):
            ref = block(k, phase, layer, at[axis], half)
            r_sem = first_sem.at[q, s, way] if which == 0 else rest_sem.at[q, s]
            send(ref, ref, near(axis, 1 if way == 0 else 3), send_sem.at[q, s], r_sem)

    def relay(k, phase, layer):
        axis = ORDERS[k][phase]
        q, s = sems(k, phase, layer)
        for way in (0, 1):
            source = (at[axis] + (3 if way == 0 else 1)) % 4
            ref = block(k, phase, layer, source, way)
            wait_bytes(ref, first_sem.at[q, s, way])
            send(
                ref, ref, near(axis, 1 if way == 0 else 3),
                send_sem.at[q, s], rest_sem.at[q, s],
            )

    def span(k, phase, layer, count):
        if phase == 2:
            return w.at[layer, k, 0, pl.ds(0, count)]
        if phase == 0:
            return w.at[:, k, 0, 0, 0, pl.ds(0, count)]
        return w.at[:, k, 0, 0, pl.ds(0, count)]

    def rest(k, phase, layer):
        q, s = sems(k, phase, layer)
        wait_bytes(span(k, phase, layer, 2), rest_sem.at[q, s])

    for k in range(3):
        loads[k].wait()
        own_half(k, 0, 0, 0)
        own_half(k, 0, 0, 1)

    for step in (1, 3, 2):
        other = (x + step) % 4
        send(
            tokens.at[other], x_buf.at[pl.ds(LOCAL, LOCAL), own_cols], (sp, other),
            tok_sem.at[0], tok_sem.at[1],
        )
    for load in loads[3:]:
        load.wait()
    for step in (1, 3, 2):
        other = (x + step) % 4
        send(vec_all.at[x], vec_all.at[x], (sp, other), par_sem.at[0], par_sem.at[1])
        send(tap_all.at[x], tap_all.at[x], (sp, other), par_sem.at[2], par_sem.at[3])

    for k in range(3):
        relay(k, 0, 0)
    for k in range(3):
        rest(k, 0, 0)
        own_half(k, 1, 0, 0)
        own_half(k, 1, 0, 1)

    own_rows = pl.ds(LOCAL, LOCAL)
    wait_bytes(x_buf.at[own_rows, pl.ds(0, 768)], tok_sem.at[1])
    send(x_buf.at[own_rows], x_buf.at[pl.ds(2 * LOCAL, LOCAL)], before, tok_sem.at[2], tok_sem.at[3])
    send(x_buf.at[own_rows], x_buf.at[pl.ds(0, LOCAL)], after, tok_sem.at[4], tok_sem.at[5])

    for k in range(3):
        relay(k, 1, 0)
    for k in range(3):
        rest(k, 1, 0)
        own_half(k, 2, 0, 0)
    for k in range(3):
        own_half(k, 2, 0, 1)
    for k in range(3):
        own_half(k, 2, 1, 0)

    def to_sibling(k, layer, index):
        ref = w.at[layer, k, c, index]
        send(ref, ref, sibling, sib_send.at[layer, k], sib_recv.at[layer, k])

    def advance(layer):
        for k in range(3):
            relay(k, 2, layer)
        for k in range(3):
            if layer + 1 < LAYERS:
                own_half(k, 2, layer + 1, 1)
        for k in range(3):
            if layer + 2 < LAYERS:
                own_half(k, 2, layer + 2, 0)
        for k in range(3):
            to_sibling(k, layer, at[ORDERS[k][2]])

    def finish(layer):
        for k in range(3):
            rest(k, 2, layer)
            for step in (1, 2, 3):
                to_sibling(k, layer, (at[ORDERS[k][2]] + step) % 4)

    def arrived(layer):
        for k in range(3):
            wait_bytes(w.at[layer, k, 0], sib_recv.at[layer, k])

    def weight(layer, k, bz, cols):
        def piece(by, bc, bx):
            index = {"x": bx, "y": by, "z": bz}
            d1, d2, d3 = ORDERS[k]
            return w[layer, k, bc, index[d3], index[d2], index[d1]]

        return jnp.concatenate(
            [
                jnp.concatenate([piece(by, bc, bx) for by in range(4) for bc in range(2)], axis=0)
                for bx in cols
            ],
            axis=1,
        )

    def compute(layer):
        r0 = STEP * layer
        n = ROWS - 2 * r0
        m = n - 2 * STEP
        xs = x_buf[pl.ds(r0, n), :].astype(F32)
        scale = lax.rsqrt(jnp.mean(xs * xs, axis=-1, keepdims=True) + EPS)
        nb[pl.ds(0, n), :] = (xs * scale * norm_gain[pl.ds(layer, 1), :]).astype(BF16)
        token = sp * LOCAL - LOCAL + r0 + lax.broadcasted_iota(jnp.int32, (n, 256), 0)
        inside = jnp.logical_and(token >= 0, token < 32 * LOCAL)
        for half in range(2):
            cols = (2 * half, 2 * half + 1)
            val = jnp.zeros((n, 256), F32)
            gate = jnp.zeros((n, 256), F32)
            for bz in range(4):
                left = nb[pl.ds(0, n), pl.ds(bz * 256, 256)]
                val = val + jnp.dot(left, weight(layer, 0, bz, cols), preferred_element_type=F32)
                gate = gate + jnp.dot(left, weight(layer, 1, bz, cols), preferred_element_type=F32)
            gated = (val * jax.nn.sigmoid(gate)).astype(BF16).astype(F32)
            g_buf[pl.ds(0, n), pl.ds(half * 256, 256)] = jnp.where(inside, gated, 0.0)
        for bx in range(4):
            lanes = pl.ds(bx * 128, 128)
            g = g_buf[pl.ds(0, n), lanes]
            total = jnp.zeros((m, 128), F32) + vec_all[bx, 0, pl.ds(layer, 1), :]
            for shift in range(8):
                moved = g if shift == 0 else pltpu.roll(g, n - shift, 0)
                for k in range(TAPS):
                    if (k + 1) % 8 == shift:
                        base = (k + 1) // 8 * 8
                        total = total + moved[base : base + m] * tap_all[bx, k, pl.ds(layer, 1), :]
            c_buf[pl.ds(0, m), lanes] = total
        conv = c_buf[pl.ds(0, m), :]
        mean = jnp.mean(conv, axis=-1, keepdims=True)
        centred = conv - mean
        spread = jnp.mean(centred * centred, axis=-1, keepdims=True)
        gain = jnp.concatenate([vec_all[bx, 1, pl.ds(layer, 1), :] for bx in range(4)], axis=1)
        shift = jnp.concatenate([vec_all[bx, 2, pl.ds(layer, 1), :] for bx in range(4)], axis=1)
        normalized = centred * lax.rsqrt(spread + EPS) * gain + shift
        act = jax.nn.silu(normalized).astype(BF16)
        rows = pl.ds(r0 + STEP, m)
        for bz in range(4):
            branch = lax.dot_general(
                act, weight(layer, 2, bz, range(4)), (((1,), (1,)), ((), ())),
                preferred_element_type=F32,
            )
            lanes = pl.ds(bz * 256, 256)
            x_buf[rows, lanes] = (x_buf[rows, lanes].astype(F32) + branch).astype(BF16)

    advance(0)
    finish(0)
    advance(1)
    wait_bytes(vec_all.at[pl.ds(0, 3)], par_sem.at[1])
    wait_bytes(tap_all.at[pl.ds(0, 3)], par_sem.at[3])
    wait_bytes(x_buf.at[own_rows], tok_sem.at[2])
    wait_bytes(x_buf.at[own_rows], tok_sem.at[3])
    wait_bytes(x_buf.at[own_rows], tok_sem.at[4])
    wait_bytes(x_buf.at[own_rows], tok_sem.at[5])
    arrived(0)
    compute(0)
    advance(2)
    finish(1)
    arrived(1)
    compute(1)
    advance(3)
    finish(2)
    arrived(2)
    compute(2)
    finish(3)
    arrived(3)
    compute(3)

    for step in (1, 3, 2):
        other = (x + step) % 4
        cols = pl.ds(pl.multiple_of(other * 256, 256), 256)
        send(x_buf.at[own_rows, cols], out.at[x], (sp, other), end_sem.at[0], end_sem.at[1])
    out[x] = x_buf[own_rows, own_cols]

    for k in range(3):
        for phase in range(2):
            wait_bytes(span(k, phase, 0, 3), send_sem.at[k, phase])
        for layer in range(LAYERS):
            wait_bytes(span(k, 2, layer, 3), send_sem.at[k, 2 + layer])
            wait_bytes(w.at[layer, k, 0], sib_send.at[layer, k])
    wait_bytes(out.at[pl.ds(0, 3)], tok_sem.at[0])
    wait_bytes(vec_all.at[pl.ds(0, 3)], par_sem.at[0])
    wait_bytes(tap_all.at[pl.ds(0, 3)], par_sem.at[2])
    wait_bytes(out.at[pl.ds(0, 3)], end_sem.at[0])
    wait_bytes(out.at[pl.ds(0, 3)], end_sem.at[1])


def shards(tokens, norm_gain, val_w, gate_w, taps, bias, ln_gain, ln_shift, out_w):
    hbm = pl.BlockSpec(memory_space=pl.ANY)
    vmem = pl.BlockSpec(memory_space=pltpu.VMEM)
    dma = pltpu.SemaphoreType.DMA
    return pl.pallas_call(
        kernel,
        out_shape=jax.ShapeDtypeStruct(tokens.shape, BF16),
        in_specs=[hbm, vmem] + [hbm] * 7,
        out_specs=vmem,
        scratch_shapes=[
            pltpu.VMEM((LAYERS, 3, 2, 4, 4, 4, 32, 128), BF16),
            pltpu.VMEM((ROWS, 1024), BF16),
            pltpu.VMEM((ROWS, 512), F32),
            pltpu.VMEM((ROWS, 512), F32),
            pltpu.VMEM((ROWS, 1024), BF16),
            pltpu.VMEM((4, TAPS, LAYERS, 128), F32),
            pltpu.VMEM((4, 3, LAYERS, 128), F32),
            dma((8,)),
            dma((3, 6)),
            dma((3, 6, 2)),
            dma((3, 6)),
            dma((LAYERS, 3)),
            dma((LAYERS, 3)),
            dma((6,)),
            dma((4,)),
            dma((2,)),
        ],
        compiler_params=pltpu.CompilerParams(collective_id=0, has_side_effects=True),
    )(
        tokens, norm_gain, val_w, gate_w, jnp.swapaxes(out_w, 1, 2),
        jnp.swapaxes(taps, 0, 1), bias, ln_gain, ln_shift,
    )


def solution(mesh):
    return jax.shard_map(
        shards,
        mesh=mesh,
        in_specs=(
            P(None, "sp", "tp"),
            P(),
            P(None, "sp", "tp"),
            P(None, "sp", "tp"),
            P(None, None, "tp"),
            P(None, "tp"),
            P(None, "tp"),
            P(None, "tp"),
            P(None, "tp", "sp"),
        ),
        out_specs=P(None, "sp", "tp"),
        check_vma=False,
    )
```

time: 455 us -> 58.6 us (0.13)
  blocking collectives: 376 us -> 0 us
  Pallas kernels: 0 us -> 56.9 us
  starting transfers between devices: 24.3 us -> 0 us
  waiting for transfers between devices: 18.1 us -> 0 us
  between operations: 13.5 us -> 0.01 us
  other arithmetic: 8.4 us -> 0 us
  matrix products: 7 us -> 0 us
    all_gather x16 -> x0, blocking collectives: 348 us -> none  [the longest x8 198 us: over_all(): lax.all_gather(a, axis, axis=dim, tiled=True)]
    pallas_call x0 -> x1, Pallas kernels: none -> 56.9 us  [shards(): pl.pallas_call(kernel, out_shape=jax.ShapeDtypeStruct(tokens.shape, BF16)...]
    psum x4 -> x0, blocking collectives: 28.6 us -> none  [together(): subtotal = lax.psum(jnp.concatenate([a.ravel() for a in arrays]), axis)]
    ppermute x8 -> x0, starting transfers between devices: 24.1 us -> none  [the longest x4 15.7 us: with_halo(): before = lax.ppermute(last, axis, up)]
    reduce_scatter x4 -> x0, waiting for transfers between devices: 18 us -> none  [shards(): lax.psum_scatter(partial_terms.reshape(num_seqs, local_len, full_width).a...]
    dot_general x12 -> x0, matrix products: 7 us -> none  [the longest x4 4.66 us: project_rows(): return jnp.dot(left_rows, shard_piece, preferred_element_type=jnp.float32)]
    convert_element_type x12 -> x0, other arithmetic: 5.28 us -> none  [the longest x4 4.41 us: shards(): stream = (stream.astype(jnp.float32) + summed).astype(jnp.bfloat16)]
  transfers between devices with their start and end apart: 12 -> 0, of which waited for: 1 -> 0; matrix products, arithmetic and copies ran while one was open for 0% -> 0% of each run, Pallas kernels for 0% -> 0%
where the time goes in v1:
time: 58.6 us; the launch traced here: 58.4 us
  Pallas kernels  56.9 us (97%)
  local copies, waits for them, and re-layouts  1.57 us (3%)
    pallas_call x1, Pallas kernels, shards(): pl.pallas_call(kernel, out_shape=jax.ShapeDtypeStruct(tokens.shape, BF16)...  56.9 us
    unnamed x1, local copies, waits for them, and re-layouts  1.57 us

profile of v1, /device:TPU:1, one launch (start us, length us, event | category | flops | bytes accessed | tf_op | source)
XLA Modules:
  0.0 58.4 jit_solution(13818723565824425845)
XLA Ops:
  0.0 56.9 %shard_map.91 = bf16[4,64,256]{2,1,0:T(8,128)(2,1)} custom-call(bf16[4,64,256]{2,1,0:T(8,128)(2,1)} %tokens.1, f32[4,1024]{1,0:T(4,128)} %norm_gain.1, bf16[4,32,128]{2,1,0:T(8,128)(2,1)} %val_w.1, bf16[4,32,128]{2,1,0:T(8,128)(2,1)} %gate_w.1, bf16[4,32,128]{2,1,0:T(8,128)(2,1)} %bitcast.3, f32[31,4,128]{2,1,0:T(4,128)} %bitcast.2, f32[4,128]{1,0:T(4,128)} %bias.1, ...), custom_call_target="tpu_custom_call" | custom-call | tf_op jit(solution)/shard_map/pallas_call | solution.py:297
  56.9 1.6 %copy.11 = bf16[4,64,256]{2,1,0:T(8,128)(2,1)} copy(bf16[4,64,256]{2,1,0:T(8,128)(2,1)} %shard_map.91) | data formatting | bytes 262144

commit v2 on v1

v2 whole, which is shorter than its diff:
```python
import jax
import jax.numpy as jnp
from jax import lax
from jax.experimental import pallas as pl
from jax.experimental.pallas import tpu as pltpu
from jax.sharding import PartitionSpec as P

MESH = pl.DeviceIdType.MESH
LAYERS = 4
TAPS = 31
EPS = 1e-6
LOCAL = 64
ROWS = 192
STEP = 16
ORDERS = (("x", "y", "z"), ("y", "z", "x"), ("z", "x", "y"))
SEMS = 200
F32 = jnp.float32
BF16 = jnp.bfloat16


def kernel(
    tokens, norm_gain, val_w, gate_w, out_w, taps, bias, ln_gain, ln_shift, out,
    w, x_buf, g_buf, c_buf, nb, gains, tap_in, tap_bf, tap_all, vec_all, y_buf, sem,
):
    sp = lax.axis_index("sp")
    x = lax.axis_index("tp")
    z = sp // 8
    y = (sp // 2) % 4
    c = sp % 2
    at = {"x": x, "y": y, "z": z}
    sibling = (sp + 1 - 2 * c, x)
    used = []

    def new_sem():
        used.append(0)
        return sem.at[len(used) - 1]

    def near(axis, step):
        if axis == "x":
            return (sp, (x + step) % 4)
        if axis == "y":
            return (z * 8 + ((y + step) % 4) * 2 + c, x)
        return (((z + step) % 4) * 8 + y * 2 + c, x)

    before = ((sp + 31) % 32, x)
    after = ((sp + 1) % 32, x)
    outer = ((sp + 31 + 2 * c) % 32, x)

    def send(ref, dst, peer, s_sem, r_sem):
        pltpu.make_async_remote_copy(
            src_ref=ref, dst_ref=dst, send_sem=s_sem, recv_sem=r_sem,
            device_id=peer, device_id_type=MESH,
        ).start()

    def wait_bytes(ref, a_sem):
        pltpu.make_async_copy(ref, ref, a_sem).wait()

    sent = []

    own_cols = pl.ds(pl.multiple_of(x * 256, 256), 256)
    own_rows = pl.ds(LOCAL, LOCAL)

    def load(src, dst):
        copy = pltpu.make_async_copy(src, dst, new_sem())
        copy.start()
        return copy

    loads = []
    for k, array in enumerate((val_w, gate_w, out_w)):
        d1, d2, d3 = ORDERS[k]
        loads.append(load(array, w.at[:, k, c, at[d3], at[d2], at[d1]]))
    tap_load = load(taps, tap_in)
    small_loads = [
        load(array, vec_all.at[x, j]) for j, array in enumerate((bias, ln_gain, ln_shift))
    ]
    token_load = load(tokens.at[x], x_buf.at[own_rows, own_cols])
    gain_load = load(norm_gain, gains)

    barrier = pltpu.get_barrier_semaphore()
    peers = [near(a, s) for a in "xyz" for s in (1, 3, 2)] + [sibling, outer]
    for peer in peers:
        pl.semaphore_signal(barrier, inc=1, device_id=peer, device_id_type=MESH)

    tap_load.wait()
    for layer in range(LAYERS):
        tap_bf[x, layer] = jnp.concatenate(
            [tap_in[:, layer, :], jnp.zeros((1, 128), F32)], axis=0
        ).astype(BF16)
    for k in range(3):
        loads[k].wait()
    pl.semaphore_wait(barrier, len(peers))

    def block(k, phase, layer, index):
        d1, d2, d3 = ORDERS[k]
        if phase == 0:
            return w.at[layer, k, c, at[d3], at[d2], index]
        if phase == 1:
            return w.at[layer, k, c, at[d3], index]
        return w.at[layer, k, c, index]

    def many(k, phase, layer, count):
        if phase == 0:
            return w.at[layer, k, 0, 0, 0, pl.ds(0, count)]
        if phase == 1:
            return w.at[layer, k, 0, 0, pl.ds(0, count)]
        return w.at[layer, k, 0, pl.ds(0, count)]

    def direct(phase, layer):
        waits = []
        for k in range(3):
            s_sem, r_sem = new_sem(), new_sem()
            axis = ORDERS[k][phase]
            ref = block(k, phase, layer, at[axis])
            for step in (2, 1, 3):
                send(ref, ref, near(axis, step), s_sem, r_sem)
            sent.append((many(k, phase, layer, 3), s_sem))
            waits.append((many(k, phase, layer, 3), r_sem))

        def wait():
            for ref, r_sem in waits:
                wait_bytes(ref, r_sem)

        return wait

    first_sems = [[[new_sem(), new_sem()] for k in range(3)] for l in range(LAYERS)]
    second_sems = [[new_sem() for k in range(3)] for l in range(LAYERS)]
    relay_sems = [[new_sem() for k in range(3)] for l in range(LAYERS)]
    ring_send = [[new_sem() for k in range(3)] for l in range(LAYERS)]
    sib_send = [[new_sem() for k in range(3)] for l in range(LAYERS)]
    sib_recv = [[new_sem() for k in range(3)] for l in range(LAYERS)]
    for l in range(LAYERS):
        for k in range(3):
            sent.append((many(k, 2, l, 3), ring_send[l][k]))
            sent.append((many(k, 2, l, 4), sib_send[l][k]))

    def half_block(k, layer, index, half):
        return w.at[layer, k, c, index, pl.ds(2 * half, 2)]

    def to_sibling(k, layer, ref):
        send(ref, ref, sibling, sib_send[layer][k], sib_recv[layer][k])

    def own(layer, which):
        for k in range(3):
            axis = ORDERS[k][2]
            for way in (0, 1):
                half = which if way == 0 else 1 - which
                ref = half_block(k, layer, at[axis], half)
                r_sem = first_sems[layer][k][way] if which == 0 else second_sems[layer][k]
                send(ref, ref, near(axis, 1 if way == 0 else 3), ring_send[layer][k], r_sem)

    def relay(layer):
        for k in range(3):
            axis = ORDERS[k][2]
            for way in (0, 1):
                step = 1 if way == 0 else 3
                ref = half_block(k, layer, (at[axis] + 4 - step) % 4, way)
                wait_bytes(ref, first_sems[layer][k][way])
                send(ref, ref, near(axis, step), ring_send[layer][k], relay_sems[layer][k])

    def share_own(layer):
        for k in range(3):
            to_sibling(k, layer, block(k, 2, layer, at[ORDERS[k][2]]))

    def share_first(layer):
        for k in range(3):
            axis = ORDERS[k][2]
            for way in (0, 1):
                to_sibling(k, layer, half_block(k, layer, (at[axis] + (3, 1)[way]) % 4, way))

    def share_second(layer):
        for k in range(3):
            axis = ORDERS[k][2]
            wait_bytes(many(k, 2, layer, 1), second_sems[layer][k])
            for way in (0, 1):
                to_sibling(k, layer, half_block(k, layer, (at[axis] + (3, 1)[way]) % 4, 1 - way))

    def share_relay(layer):
        for k in range(3):
            axis = ORDERS[k][2]
            wait_bytes(many(k, 2, layer, 1), relay_sems[layer][k])
            to_sibling(k, layer, block(k, 2, layer, (at[axis] + 2) % 4))

    def arrived(layer):
        for k in range(3):
            wait_bytes(many(k, 2, layer, 4), sib_recv[layer][k])

    def weight(layer, k, bz, cols):
        def piece(by, bc, bx):
            index = {"x": bx, "y": by, "z": bz}
            d1, d2, d3 = ORDERS[k]
            return w[layer, k, bc, index[d3], index[d2], index[d1]]

        return jnp.concatenate(
            [
                jnp.concatenate([piece(by, bc, bx) for by in range(4) for bc in range(2)], axis=0)
                for bx in cols
            ],
            axis=1,
        )

    def branch(layer, act, bz):
        return lax.dot_general(
            act, weight(layer, 2, bz, range(4)), (((1,), (1,)), ((), ())),
            preferred_element_type=F32,
        )

    def activated(layer):
        r0 = STEP * layer
        n = ROWS - 2 * r0
        m = n - 2 * STEP
        xs = x_buf[pl.ds(r0, n), :].astype(F32)
        scale = lax.rsqrt(jnp.mean(xs * xs, axis=-1, keepdims=True) + EPS)
        nb[pl.ds(0, n), :] = (xs * scale * gains[pl.ds(layer, 1), :]).astype(BF16)
        token = sp * LOCAL - LOCAL + r0 + lax.broadcasted_iota(jnp.int32, (n, 256), 0)
        inside = jnp.logical_and(token >= 0, token < 32 * LOCAL)
        for half in range(2):
            cols = (2 * half, 2 * half + 1)
            val = jnp.zeros((n, 256), F32)
            gate = jnp.zeros((n, 256), F32)
            for bz in range(4):
                left = nb[pl.ds(0, n), pl.ds(bz * 256, 256)]
                val = val + jnp.dot(left, weight(layer, 0, bz, cols), preferred_element_type=F32)
                gate = gate + jnp.dot(left, weight(layer, 1, bz, cols), preferred_element_type=F32)
            gated = (val * jax.nn.sigmoid(gate)).astype(BF16).astype(F32)
            g_buf[pl.ds(0, n), pl.ds(half * 256, 256)] = jnp.where(inside, gated, 0.0)
        for bx in range(4):
            lanes = pl.ds(bx * 128, 128)
            g = g_buf[pl.ds(0, n), lanes]
            total = jnp.zeros((m, 128), F32) + vec_all[bx, 0, pl.ds(layer, 1), :]
            for shift in range(8):
                moved = g if shift == 0 else pltpu.roll(g, n - shift, 0)
                for k in range(TAPS):
                    if (k + 1) % 8 == shift:
                        base = (k + 1) // 8 * 8
                        total = total + moved[base : base + m] * tap_all[bx, layer, pl.ds(k, 1), :]
            c_buf[pl.ds(0, m), lanes] = total
        conv = c_buf[pl.ds(0, m), :]
        mean = jnp.mean(conv, axis=-1, keepdims=True)
        centred = conv - mean
        spread = jnp.mean(centred * centred, axis=-1, keepdims=True)
        gain = jnp.concatenate([vec_all[bx, 1, pl.ds(layer, 1), :] for bx in range(4)], axis=1)
        shift = jnp.concatenate([vec_all[bx, 2, pl.ds(layer, 1), :] for bx in range(4)], axis=1)
        normalized = centred * lax.rsqrt(spread + EPS) * gain + shift
        return jax.nn.silu(normalized).astype(BF16)

    def compute(layer):
        act = activated(layer)
        rows = pl.ds(STEP * (layer + 1), ROWS - 2 * STEP * (layer + 1))
        for bz in range(4):
            lanes = pl.ds(bz * 256, 256)
            x_buf[rows, lanes] = (x_buf[rows, lanes].astype(F32) + branch(layer, act, bz)).astype(BF16)

    ph0_first = direct(0, pl.ds(0, 1))
    ph0_later = direct(0, pl.ds(1, 3))

    tok_send, tok_recv = new_sem(), new_sem()
    for step in (2, 1, 3):
        other = (x + step) % 4
        send(tokens.at[other], x_buf.at[own_rows, own_cols], (sp, other), tok_send, tok_recv)
    sent.append((x_buf.at[own_rows, pl.ds(0, 768)], tok_send))
    own_taps = pl.ds(2 * c, 2)
    par_sems = [new_sem() for _ in range(6)]
    for copy in small_loads:
        copy.wait()
    for step in (2, 1, 3):
        other = (x + step) % 4
        send(tap_bf.at[x, own_taps], tap_bf.at[x, own_taps], (sp, other), par_sems[0], par_sems[1])
        send(vec_all.at[x], vec_all.at[x], (sp, other), par_sems[2], par_sems[3])
    sent.append((tap_bf.at[pl.ds(0, 3), pl.ds(0, 2)], par_sems[0]))
    sent.append((vec_all.at[pl.ds(0, 3)], par_sems[2]))

    ph0_first()
    ph1 = [direct(1, pl.ds(0, 1))]
    ph0_later()
    ph1.append(direct(1, pl.ds(1, 1)))
    ph1.append(direct(1, pl.ds(2, 1)))
    ph1.append(direct(1, pl.ds(3, 1)))

    token_load.wait()
    wait_bytes(x_buf.at[own_rows, pl.ds(0, 768)], tok_recv)
    halo = [new_sem() for _ in range(4)]
    send(x_buf.at[own_rows], x_buf.at[pl.ds(2 * LOCAL, LOCAL)], before, halo[0], halo[1])
    send(x_buf.at[own_rows], x_buf.at[pl.ds(0, LOCAL)], after, halo[2], halo[3])
    wait_bytes(tap_bf.at[pl.ds(0, 3), pl.ds(0, 2)], par_sems[1])
    for step in (1, 2, 3):
        other = (x + step) % 4
        ref = tap_bf.at[other, own_taps]
        send(ref, ref, sibling, par_sems[4], par_sems[5])
    sent.append((tap_bf.at[pl.ds(0, 3), pl.ds(0, 2)], par_sems[4]))

    ph1[0]()
    own(0, 0)
    own(0, 1)
    share_own(0)
    ph1[1]()
    own(1, 0)
    relay(0)
    share_first(0)
    own(1, 1)
    share_own(1)
    ph1[2]()
    own(2, 0)
    share_second(0)
    share_relay(0)
    relay(1)
    share_first(1)
    own(2, 1)
    share_own(2)
    ph1[3]()
    own(3, 0)

    wait_bytes(vec_all.at[pl.ds(0, 3)], par_sems[3])
    wait_bytes(tap_bf.at[pl.ds(0, 3), pl.ds(0, 2)], par_sems[5])
    tap_all[...] = tap_bf[...].astype(F32)
    gain_load.wait()
    for a_sem in halo:
        wait_bytes(x_buf.at[own_rows], a_sem)

    arrived(0)
    compute(0)
    share_second(1)
    share_relay(1)
    relay(2)
    share_first(2)
    own(3, 1)
    share_own(3)
    arrived(1)
    compute(1)
    share_second(2)
    share_relay(2)
    relay(3)
    share_first(3)
    arrived(2)
    compute(2)
    share_second(3)
    share_relay(3)
    arrived(3)

    act = activated(3)
    end_send, end_recv = new_sem(), new_sem()
    for i, step in enumerate((2, 1, 3, 0)):
        other = (x + step) % 4
        cols = pl.ds(pl.multiple_of(other * 256, 256), 256)
        result = (x_buf[own_rows, cols].astype(F32) + branch(3, act, other)).astype(BF16)
        if step:
            y_buf[i] = result
            send(y_buf.at[i], out.at[x], (sp, other), end_send, end_recv)
        else:
            out[x] = result
    sent.append((y_buf.at[pl.ds(0, 3)], end_send))
    wait_bytes(y_buf.at[pl.ds(0, 3)], end_recv)
    for ref, a_sem in sent:
        wait_bytes(ref, a_sem)


def shards(tokens, norm_gain, val_w, gate_w, taps, bias, ln_gain, ln_shift, out_w):
    hbm = pl.BlockSpec(memory_space=pl.ANY)
    vmem = pl.BlockSpec(memory_space=pltpu.VMEM)
    return pl.pallas_call(
        kernel,
        out_shape=pltpu.VMEM(tokens.shape, BF16),
        in_specs=[hbm] * 9,
        out_specs=vmem,
        scratch_shapes=[
            pltpu.VMEM((LAYERS, 3, 2, 4, 4, 4, 32, 128), BF16),
            pltpu.VMEM((ROWS, 1024), BF16),
            pltpu.VMEM((ROWS, 512), F32),
            pltpu.VMEM((ROWS, 512), F32),
            pltpu.VMEM((ROWS, 1024), BF16),
            pltpu.VMEM((LAYERS, 1024), F32),
            pltpu.VMEM((TAPS, LAYERS, 128), F32),
            pltpu.VMEM((4, LAYERS, 32, 128), BF16),
            pltpu.VMEM((4, LAYERS, 32, 128), F32),
            pltpu.VMEM((4, 3, LAYERS, 128), F32),
            pltpu.VMEM((3, LOCAL, 256), BF16),
            pltpu.SemaphoreType.DMA((SEMS,)),
        ],
        compiler_params=pltpu.CompilerParams(collective_id=0, has_side_effects=True),
    )(
        tokens, norm_gain, val_w, gate_w, jnp.swapaxes(out_w, 1, 2),
        jnp.swapaxes(taps, 0, 1), bias, ln_gain, ln_shift,
    )


def solution(mesh):
    return jax.shard_map(
        shards,
        mesh=mesh,
        in_specs=(
            P(None, "sp", "tp"),
            P(),
            P(None, "sp", "tp"),
            P(None, "sp", "tp"),
            P(None, None, "tp"),
            P(None, "tp"),
            P(None, "tp"),
            P(None, "tp"),
            P(None, "tp", "sp"),
        ),
        out_specs=P(None, "sp", "tp"),
        check_vma=False,
    )
```

time: 58.6 us -> 48.2 us (0.82)
  Pallas kernels: 56.9 us -> 47.4 us
  local copies, waits for them, and re-layouts: 1.57 us -> 0.66 us
    pallas_call x1, Pallas kernels: 56.9 us -> 47.4 us  [shards(): pl.pallas_call(kernel, out_shape=pltpu.VMEM(tokens.shape, BF16), in_specs...]
    unnamed x1, local copies, waits for them, and re-layouts: 1.57 us -> 0.66 us
where the time goes in v2:
time: 48.2 us; the launch traced here: 48.1 us
  Pallas kernels  47.4 us (98%)
  local copies, waits for them, and re-layouts  0.66 us (1%)
    pallas_call x1, Pallas kernels, shards(): pl.pallas_call(kernel, out_shape=pltpu.VMEM(tokens.shape, BF16), in_specs...  47.4 us

profile of v2, /device:TPU:1, one launch (start us, length us, event | category | flops | bytes accessed | tf_op | source)
XLA Modules:
  0.0 48.1 jit_solution(7552146854377488766)
XLA Ops:
  0.0 47.4 %shard_map.91 = bf16[4,64,256]{2,1,0:T(8,128)(2,1)S(1)} custom-call(bf16[4,64,256]{2,1,0:T(8,128)(2,1)} %tokens.1, f32[4,1024]{1,0:T(4,128)} %norm_gain.1, bf16[4,32,128]{2,1,0:T(8,128)(2,1)} %val_w.1, bf16[4,32,128]{2,1,0:T(8,128)(2,1)} %gate_w.1, bf16[4,32,128]{2,1,0:T(8,128)(2,1)} %bitcast.3, f32[31,4,128]{2,1,0:T(4,128)} %bitcast.2, f32[4,128]{1,0:T(4,128)} %bias.1, ...), custom_call_target="tpu_custom_call" | custom-call | tf_op jit(solution)/shard_map/pallas_call | solution.py:359
  47.4 0.7 %copy.11 = bf16[4,64,256]{2,1,0:T(8,128)(2,1)} copy(bf16[4,64,256]{2,1,0:T(8,128)(2,1)S(1)} %shard_map.91) | data formatting | bytes 262144

commit v3 on v2

--- a/solution.py
+++ b/solution.py
@@ -12,8 +12,9 @@
 LOCAL = 64
 ROWS = 192
 STEP = 16
-ORDERS = (("x", "y", "z"), ("y", "z", "x"), ("z", "x", "y"))
-SEMS = 200
+CYCLE = ("xyz", "yzx", "zxy")
+ORDERS = (CYCLE, CYCLE, CYCLE, CYCLE)
+SEMS = 280
 F32 = jnp.float32
 BF16 = jnp.bfloat16
 
@@ -66,9 +67,10 @@
         return copy
 
     loads = []
-    for k, array in enumerate((val_w, gate_w, out_w)):
-        d1, d2, d3 = ORDERS[k]
-        loads.append(load(array, w.at[:, k, c, at[d3], at[d2], at[d1]]))
+    for layer in range(LAYERS):
+        for k, array in enumerate((val_w, gate_w, out_w)):
+            d1, d2, d3 = ORDERS[layer][k]
+            loads.append(load(array.at[layer], w.at[layer, k, c, at[d3], at[d2], at[d1]]))
     tap_load = load(taps, tap_in)
     small_loads = [
         load(array, vec_all.at[x, j]) for j, array in enumerate((bias, ln_gain, ln_shift))
@@ -86,12 +88,12 @@
         tap_bf[x, layer] = jnp.concatenate(
             [tap_in[:, layer, :], jnp.zeros((1, 128), F32)], axis=0
         ).astype(BF16)
-    for k in range(3):
-        loads[k].wait()
+    for copy in loads:
+        copy.wait()
     pl.semaphore_wait(barrier, len(peers))
 
     def block(k, phase, layer, index):
-        d1, d2, d3 = ORDERS[k]
+        d1, d2, d3 = ORDERS[layer][k]
         if phase == 0:
             return w.at[layer, k, c, at[d3], at[d2], index]
         if phase == 1:
@@ -109,7 +111,7 @@
         waits = []
         for k in range(3):
             s_sem, r_sem = new_sem(), new_sem()
-            axis = ORDERS[k][phase]
+            axis = ORDERS[layer][k][phase]
             ref = block(k, phase, layer, at[axis])
             for step in (2, 1, 3):
                 send(ref, ref, near(axis, step), s_sem, r_sem)
@@ -121,6 +123,39 @@
                 wait_bytes(ref, r_sem)
 
         return wait
+
+    line_sems = [[[new_sem(), new_sem()] for k in range(3)] for l in range(LAYERS)]
+    line_rest = [[new_sem() for k in range(3)] for l in range(LAYERS)]
+    line_send = [[new_sem() for k in range(3)] for l in range(LAYERS)]
+
+    def line_half(k, layer, index, half):
+        d1, d2, d3 = ORDERS[layer][k]
+        return w.at[layer, k, c, at[d3], index, pl.ds(2 * half, 2)]
+
+    def line_own(layer):
+        for which in (0, 1):
+            for k in range(3):
+                axis = ORDERS[layer][k][1]
+                for way in (0, 1):
+                    half = which if way == 0 else 1 - which
+                    ref = line_half(k, layer, at[axis], half)
+                    r_sem = line_sems[layer][k][way] if which == 0 else line_rest[layer][k]
+                    send(ref, ref, near(axis, 1 if way == 0 else 3), line_send[layer][k], r_sem)
+        for k in range(3):
+            sent.append((many(k, 1, layer, 3), line_send[layer][k]))
+
+    def line_relay(layer):
+        for k in range(3):
+            axis = ORDERS[layer][k][1]
+            for way in (0, 1):
+                step = 1 if way == 0 else 3
+                ref = line_half(k, layer, (at[axis] + 4 - step) % 4, way)
+                wait_bytes(ref, line_sems[layer][k][way])
+                send(ref, ref, near(axis, step), line_send[layer][k], line_rest[layer][k])
+
+    def line_wait(layer):
+        for k in range(3):
+            wait_bytes(many(k, 1, layer, 2), line_rest[layer][k])
 
     first_sems = [[[new_sem(), new_sem()] for k in range(3)] for l in range(LAYERS)]
     second_sems = [[new_sem() for k in range(3)] for l in range(LAYERS)]
@@ -141,7 +176,7 @@
 
     def own(layer, which):
         for k in range(3):
-            axis = ORDERS[k][2]
+            axis = ORDERS[layer][k][2]
             for way in (0, 1):
                 half = which if way == 0 else 1 - which
                 ref = half_block(k, layer, at[axis], half)
@@ -150,7 +185,7 @@
 
     def relay(layer):
         for k in range(3):
-            axis = ORDERS[k][2]
+            axis = ORDERS[layer][k][2]
             for way in (0, 1):
                 step = 1 if way == 0 else 3
                 ref = half_block(k, layer, (at[axis] + 4 - step) % 4, way)
@@ -159,24 +194,24 @@
 
     def share_own(layer):
         for k in range(3):
-            to_sibling(k, layer, block(k, 2, layer, at[ORDERS[k][2]]))
+            to_sibling(k, layer, block(k, 2, layer, at[ORDERS[layer][k][2]]))
 
     def share_first(layer):
         for k in range(3):
-            axis = ORDERS[k][2]
+            axis = ORDERS[layer][k][2]
             for way in (0, 1):
                 to_sibling(k, layer, half_block(k, layer, (at[axis] + (3, 1)[way]) % 4, way))
 
     def share_second(layer):
         for k in range(3):
-            axis = ORDERS[k][2]
+            axis = ORDERS[layer][k][2]
             wait_bytes(many(k, 2, layer, 1), second_sems[layer][k])
             for way in (0, 1):
                 to_sibling(k, layer, half_block(k, layer, (at[axis] + (3, 1)[way]) % 4, 1 - way))
 
     def share_relay(layer):
         for k in range(3):
-            axis = ORDERS[k][2]
+            axis = ORDERS[layer][k][2]
             wait_bytes(many(k, 2, layer, 1), relay_sems[layer][k])
             to_sibling(k, layer, block(k, 2, layer, (at[axis] + 2) % 4))
 
@@ -187,7 +222,7 @@
     def weight(layer, k, bz, cols):
         def piece(by, bc, bx):
             index = {"x": bx, "y": by, "z": bz}
-            d1, d2, d3 = ORDERS[k]
+            d1, d2, d3 = ORDERS[layer][k]
             return w[layer, k, bc, index[d3], index[d2], index[d1]]
 
         return jnp.concatenate(
@@ -204,7 +239,7 @@
             preferred_element_type=F32,
         )
 
-    def activated(layer):
+    def activated(layer, middle):
         r0 = STEP * layer
         n = ROWS - 2 * r0
         m = n - 2 * STEP
@@ -234,6 +269,7 @@
                         base = (k + 1) // 8 * 8
                         total = total + moved[base : base + m] * tap_all[bx, layer, pl.ds(k, 1), :]
             c_buf[pl.ds(0, m), lanes] = total
+        middle()
         conv = c_buf[pl.ds(0, m), :]
         mean = jnp.mean(conv, axis=-1, keepdims=True)
         centred = conv - mean
@@ -243,15 +279,14 @@
         normalized = centred * lax.rsqrt(spread + EPS) * gain + shift
         return jax.nn.silu(normalized).astype(BF16)
 
-    def compute(layer):
-        act = activated(layer)
+    def compute(layer, middle):
+        act = activated(layer, middle)
         rows = pl.ds(STEP * (layer + 1), ROWS - 2 * STEP * (layer + 1))
         for bz in range(4):
             lanes = pl.ds(bz * 256, 256)
             x_buf[rows, lanes] = (x_buf[rows, lanes].astype(F32) + branch(layer, act, bz)).astype(BF16)
 
-    ph0_first = direct(0, pl.ds(0, 1))
-    ph0_later = direct(0, pl.ds(1, 3))
+    ph0 = [direct(0, layer) for layer in range(LAYERS)]
 
     tok_send, tok_recv = new_sem(), new_sem()
     for step in (2, 1, 3):
@@ -269,12 +304,14 @@
     sent.append((tap_bf.at[pl.ds(0, 3), pl.ds(0, 2)], par_sems[0]))
     sent.append((vec_all.at[pl.ds(0, 3)], par_sems[2]))
 
-    ph0_first()
-    ph1 = [direct(1, pl.ds(0, 1))]
-    ph0_later()
-    ph1.append(direct(1, pl.ds(1, 1)))
-    ph1.append(direct(1, pl.ds(2, 1)))
-    ph1.append(direct(1, pl.ds(3, 1)))
+    ph1 = []
+    for layer in range(LAYERS):
+        ph0[layer]()
+        if layer in (2, 3):
+            line_own(layer)
+            ph1.append(lambda layer=layer: line_wait(layer))
+        else:
+            ph1.append(direct(1, layer))
 
     token_load.wait()
     wait_bytes(x_buf.at[own_rows, pl.ds(0, 768)], tok_recv)
@@ -291,20 +328,22 @@
     ph1[0]()
     own(0, 0)
     own(0, 1)
+    line_relay(2)
+    line_relay(3)
     share_own(0)
     ph1[1]()
     own(1, 0)
     relay(0)
+    own(1, 1)
     share_first(0)
-    own(1, 1)
     share_own(1)
     ph1[2]()
     own(2, 0)
+    relay(1)
+    own(2, 1)
     share_second(0)
     share_relay(0)
-    relay(1)
     share_first(1)
-    own(2, 1)
     share_own(2)
     ph1[3]()
     own(3, 0)
@@ -317,26 +356,29 @@
         wait_bytes(x_buf.at[own_rows], a_sem)
 
     arrived(0)
-    compute(0)
+
+    def middle0():
+        relay(2)
+        own(3, 1)
+
+    compute(0, lambda: None)
+    middle0()
+    share_first(2)
     share_second(1)
     share_relay(1)
-    relay(2)
-    share_first(2)
-    own(3, 1)
     share_own(3)
     arrived(1)
-    compute(1)
+    compute(1, lambda: None)
+    relay(3)
+    share_first(3)
     share_second(2)
     share_relay(2)
-    relay(3)
-    share_first(3)
     arrived(2)
-    compute(2)
-    share_second(3)
+    compute(2, lambda: share_second(3))
     share_relay(3)
     arrived(3)
 
-    act = activated(3)
+    act = activated(3, lambda: None)
     end_send, end_recv = new_sem(), new_sem()
     for i, step in enumerate((2, 1, 3, 0)):
         other = (x + step) % 4

time: 48.2 us -> 46.9 us (0.973)
  Pallas kernels: 47.4 us -> 45.9 us
    pallas_call x1, Pallas kernels: 47.4 us -> 45.9 us  [shards(): pl.pallas_call(kernel, out_shape=pltpu.VMEM(tokens.shape, BF16), in_specs...]
where the time goes in v3:
time: 46.9 us; the launch traced here: 46.5 us
  Pallas kernels  45.9 us (98%)
  local copies, waits for them, and re-layouts  0.66 us (1%)
    pallas_call x1, Pallas kernels, shards(): pl.pallas_call(kernel, out_shape=pltpu.VMEM(tokens.shape, BF16), in_specs...  45.9 us

profile of v3, /device:TPU:1, one launch (start us, length us, event | category | flops | bytes accessed | tf_op | source)
XLA Modules:
  0.0 46.5 jit_solution(2186839019894283766)
XLA Ops:
  0.0 45.9 %shard_map.91 = bf16[4,64,256]{2,1,0:T(8,128)(2,1)S(1)} custom-call(bf16[4,64,256]{2,1,0:T(8,128)(2,1)} %tokens.1, f32[4,1024]{1,0:T(4,128)} %norm_gain.1, bf16[4,32,128]{2,1,0:T(8,128)(2,1)} %val_w.1, bf16[4,32,128]{2,1,0:T(8,128)(2,1)} %gate_w.1, bf16[4,32,128]{2,1,0:T(8,128)(2,1)} %bitcast.3, f32[31,4,128]{2,1,0:T(4,128)} %bitcast.2, f32[4,128]{1,0:T(4,128)} %bias.1, ...), custom_call_target="tpu_custom_call" | custom-call | tf_op jit(solution)/shard_map/pallas_call | solution.py:401
  45.9 0.7 %copy.11 = bf16[4,64,256]{2,1,0:T(8,128)(2,1)} copy(bf16[4,64,256]{2,1,0:T(8,128)(2,1)S(1)} %shard_map.91) | data formatting | bytes 262144

commit v4 on v3

--- a/solution.py
+++ b/solution.py
@@ -239,13 +239,17 @@
             preferred_element_type=F32,
         )
 
+    def normed(layer):
+        r0 = STEP * layer
+        n = ROWS - 2 * r0
+        xs = x_buf[pl.ds(r0, n), :].astype(F32)
+        scale = lax.rsqrt(jnp.mean(xs * xs, axis=-1, keepdims=True) + EPS)
+        nb[pl.ds(0, n), :] = (xs * scale * gains[pl.ds(layer, 1), :]).astype(BF16)
+
     def activated(layer, middle):
         r0 = STEP * layer
         n = ROWS - 2 * r0
         m = n - 2 * STEP
-        xs = x_buf[pl.ds(r0, n), :].astype(F32)
-        scale = lax.rsqrt(jnp.mean(xs * xs, axis=-1, keepdims=True) + EPS)
-        nb[pl.ds(0, n), :] = (xs * scale * gains[pl.ds(layer, 1), :]).astype(BF16)
         token = sp * LOCAL - LOCAL + r0 + lax.broadcasted_iota(jnp.int32, (n, 256), 0)
         inside = jnp.logical_and(token >= 0, token < 32 * LOCAL)
         for half in range(2):
@@ -355,6 +359,7 @@
     for a_sem in halo:
         wait_bytes(x_buf.at[own_rows], a_sem)
 
+    normed(0)
     arrived(0)
 
     def middle0():
@@ -367,15 +372,18 @@
     share_second(1)
     share_relay(1)
     share_own(3)
+    normed(1)
     arrived(1)
+    relay(3)
+    share_second(2)
+    share_first(3)
     compute(1, lambda: None)
-    relay(3)
-    share_first(3)
-    share_second(2)
     share_relay(2)
+    normed(2)
     arrived(2)
     compute(2, lambda: share_second(3))
     share_relay(3)
+    normed(3)
     arrived(3)
 
     act = activated(3, lambda: None)

time: 46.9 us -> 45.7 us (0.974)
  Pallas kernels: 45.9 us -> 44.5 us
    pallas_call x1, Pallas kernels: 45.9 us -> 44.5 us  [shards(): pl.pallas_call(kernel, out_shape=pltpu.VMEM(tokens.shape, BF16), in_specs...]
where the time goes in v4:
time: 45.7 us; the launch traced here: 45.2 us
  Pallas kernels  44.5 us (97%)
  local copies, waits for them, and re-layouts  0.66 us (1%)
    pallas_call x1, Pallas kernels, shards(): pl.pallas_call(kernel, out_shape=pltpu.VMEM(tokens.shape, BF16), in_specs...  44.5 us

profile of v4, /device:TPU:1, one launch (start us, length us, event | category | flops | bytes accessed | tf_op | source)
XLA Modules:
  0.0 45.2 jit_solution(3890694949613695718)
XLA Ops:
  0.0 44.5 %shard_map.91 = bf16[4,64,256]{2,1,0:T(8,128)(2,1)S(1)} custom-call(bf16[4,64,256]{2,1,0:T(8,128)(2,1)} %tokens.1, f32[4,1024]{1,0:T(4,128)} %norm_gain.1, bf16[4,32,128]{2,1,0:T(8,128)(2,1)} %val_w.1, bf16[4,32,128]{2,1,0:T(8,128)(2,1)} %gate_w.1, bf16[4,32,128]{2,1,0:T(8,128)(2,1)} %bitcast.3, f32[31,4,128]{2,1,0:T(4,128)} %bitcast.2, f32[4,128]{1,0:T(4,128)} %bias.1, ...), custom_call_target="tpu_custom_call" | custom-call | tf_op jit(solution)/shard_map/pallas_call | solution.py:409
  44.5 0.7 %copy.11 = bf16[4,64,256]{2,1,0:T(8,128)(2,1)} copy(bf16[4,64,256]{2,1,0:T(8,128)(2,1)S(1)} %shard_map.91) | data formatting | bytes 262144

commit v5 on v4

--- a/solution.py
+++ b/solution.py
@@ -83,12 +83,7 @@
     for peer in peers:
         pl.semaphore_signal(barrier, inc=1, device_id=peer, device_id_type=MESH)
 
-    tap_load.wait()
-    for layer in range(LAYERS):
-        tap_bf[x, layer] = jnp.concatenate(
-            [tap_in[:, layer, :], jnp.zeros((1, 128), F32)], axis=0
-        ).astype(BF16)
-    for copy in loads:
+    for copy in loads[:3]:
         copy.wait()
     pl.semaphore_wait(barrier, len(peers))
 
@@ -167,12 +162,14 @@
         for k in range(3):
             sent.append((many(k, 2, l, 3), ring_send[l][k]))
             sent.append((many(k, 2, l, 4), sib_send[l][k]))
+    late_sems = [new_sem() for k in range(3)]
 
     def half_block(k, layer, index, half):
         return w.at[layer, k, c, index, pl.ds(2 * half, 2)]
 
-    def to_sibling(k, layer, ref):
-        send(ref, ref, sibling, sib_send[layer][k], sib_recv[layer][k])
+    def to_sibling(k, layer, ref, late=False):
+        r_sem = late_sems[k] if late and layer == 3 else sib_recv[layer][k]
+        send(ref, ref, sibling, sib_send[layer][k], r_sem)
 
     def own(layer, which):
         for k in range(3):
@@ -213,11 +210,11 @@
         for k in range(3):
             axis = ORDERS[layer][k][2]
             wait_bytes(many(k, 2, layer, 1), relay_sems[layer][k])
-            to_sibling(k, layer, block(k, 2, layer, (at[axis] + 2) % 4))
+            to_sibling(k, layer, block(k, 2, layer, (at[axis] + 2) % 4), late=True)
 
     def arrived(layer):
         for k in range(3):
-            wait_bytes(many(k, 2, layer, 4), sib_recv[layer][k])
+            wait_bytes(many(k, 2, layer, 3 if layer == 3 else 4), sib_recv[layer][k])
 
     def weight(layer, k, bz, cols):
         def piece(by, bc, bx):
@@ -232,6 +229,40 @@
             ],
             axis=1,
         )
+
+    def left(n, bz):
+        return nb[pl.ds(0, n), pl.ds(pl.multiple_of(bz * 256, 256), 256)]
+
+    last = ROWS - 2 * STEP * 3
+    every = pl.ds(0, last)
+
+    def gate_block(bx):
+        total = jnp.zeros((last, 128), F32)
+        for bz in range(4):
+            total = total + jnp.dot(
+                left(last, bz), weight(3, 1, bz, (bx,)), preferred_element_type=F32
+            )
+        g_buf[every, pl.ds(pl.multiple_of(bx * 128, 128), 128)] = total
+
+    def last_early():
+        total = jnp.zeros((last, 512), F32)
+        for step in (0, 1, 3):
+            bz = (z + step) % 4
+            total = total + jnp.dot(
+                left(last, bz), weight(3, 0, bz, range(4)), preferred_element_type=F32
+            )
+        c_buf[every, :] = total
+        for step in (0, 1, 3):
+            gate_block((x + step) % 4)
+
+    def last_late():
+        bz = (z + 2) % 4
+        gate_block((x + 2) % 4)
+        for half in range(2):
+            lanes = pl.ds(half * 256, 256)
+            c_buf[every, lanes] = c_buf[every, lanes] + jnp.dot(
+                left(last, bz), weight(3, 0, bz, (2 * half, 2 * half + 1)), preferred_element_type=F32
+            )
 
     def branch(layer, act, bz):
         return lax.dot_general(
@@ -254,12 +285,16 @@
         inside = jnp.logical_and(token >= 0, token < 32 * LOCAL)
         for half in range(2):
             cols = (2 * half, 2 * half + 1)
-            val = jnp.zeros((n, 256), F32)
-            gate = jnp.zeros((n, 256), F32)
-            for bz in range(4):
-                left = nb[pl.ds(0, n), pl.ds(bz * 256, 256)]
-                val = val + jnp.dot(left, weight(layer, 0, bz, cols), preferred_element_type=F32)
-                gate = gate + jnp.dot(left, weight(layer, 1, bz, cols), preferred_element_type=F32)
+            if layer == 3:
+                val = c_buf[pl.ds(0, n), pl.ds(half * 256, 256)]
+                gate = g_buf[pl.ds(0, n), pl.ds(half * 256, 256)]
+            else:
+                val = jnp.zeros((n, 256), F32)
+                gate = jnp.zeros((n, 256), F32)
+                for bz in range(4):
+                    part = left(n, bz)
+                    val = val + jnp.dot(part, weight(layer, 0, bz, cols), preferred_element_type=F32)
+                    gate = gate + jnp.dot(part, weight(layer, 1, bz, cols), preferred_element_type=F32)
             gated = (val * jax.nn.sigmoid(gate)).astype(BF16).astype(F32)
             g_buf[pl.ds(0, n), pl.ds(half * 256, 256)] = jnp.where(inside, gated, 0.0)
         for bx in range(4):
@@ -290,7 +325,15 @@
             lanes = pl.ds(bz * 256, 256)
             x_buf[rows, lanes] = (x_buf[rows, lanes].astype(F32) + branch(layer, act, bz)).astype(BF16)
 
-    ph0 = [direct(0, layer) for layer in range(LAYERS)]
+    ph0 = [direct(0, 0)]
+    for copy in loads[3:]:
+        copy.wait()
+    ph0 += [direct(0, layer) for layer in range(1, LAYERS)]
+    tap_load.wait()
+    for layer in range(LAYERS):
+        tap_bf[x, layer] = jnp.concatenate(
+            [tap_in[:, layer, :], jnp.zeros((1, 128), F32)], axis=0
+        ).astype(BF16)
 
     tok_send, tok_recv = new_sem(), new_sem()
     for step in (2, 1, 3):
@@ -381,12 +424,18 @@
     share_relay(2)
     normed(2)
     arrived(2)
-    compute(2, lambda: share_second(3))
+    share_second(3)
+    compute(2, lambda: None)
+    normed(3)
     share_relay(3)
-    normed(3)
     arrived(3)
+    last_early()
+    for k in (1, 0):
+        wait_bytes(many(k, 2, 3, 1), late_sems[k])
+    last_late()
 
     act = activated(3, lambda: None)
+    wait_bytes(many(2, 2, 3, 1), late_sems[2])
     end_send, end_recv = new_sem(), new_sem()
     for i, step in enumerate((2, 1, 3, 0)):
         other = (x + step) % 4
@@ -397,10 +446,10 @@
             send(y_buf.at[i], out.at[x], (sp, other), end_send, end_recv)
         else:
             out[x] = result
-    sent.append((y_buf.at[pl.ds(0, 3)], end_send))
-    wait_bytes(y_buf.at[pl.ds(0, 3)], end_recv)
     for ref, a_sem in sent:
         wait_bytes(ref, a_sem)
+    wait_bytes(y_buf.at[pl.ds(0, 3)], end_send)
+    wait_bytes(y_buf.at[pl.ds(0, 3)], end_recv)
 
 
 def shards(tokens, norm_gain, val_w, gate_w, taps, bias, ln_gain, ln_shift, out_w):

time: 45.7 us -> 45.5 us (level)
  no operation moved by 1% of the time
where the time goes in v5:
time: 45.5 us; the launch traced here: 45.1 us
  Pallas kernels  44.5 us (98%)
  local copies, waits for them, and re-layouts  0.66 us (1%)
    pallas_call x1, Pallas kernels, shards(): pl.pallas_call(kernel, out_shape=pltpu.VMEM(tokens.shape, BF16), in_specs...  44.5 us

profile of v5, /device:TPU:1, one launch (start us, length us, event | category | flops | bytes accessed | tf_op | source)
XLA Modules:
  0.0 45.1 jit_solution(2755290679230322151)
XLA Ops:
  0.0 44.5 %shard_map.91 = bf16[4,64,256]{2,1,0:T(8,128)(2,1)S(1)} custom-call(bf16[4,64,256]{2,1,0:T(8,128)(2,1)} %tokens.1, f32[4,1024]{1,0:T(4,128)} %norm_gain.1, bf16[4,32,128]{2,1,0:T(8,128)(2,1)} %val_w.1, bf16[4,32,128]{2,1,0:T(8,128)(2,1)} %gate_w.1, bf16[4,32,128]{2,1,0:T(8,128)(2,1)} %bitcast.3, f32[31,4,128]{2,1,0:T(4,128)} %bitcast.2, f32[4,128]{1,0:T(4,128)} %bias.1, ...), custom_call_target="tpu_custom_call" | custom-call | tf_op jit(solution)/shard_map/pallas_call | solution.py:458
  44.5 0.7 %copy.11 = bf16[4,64,256]{2,1,0:T(8,128)(2,1)} copy(bf16[4,64,256]{2,1,0:T(8,128)(2,1)S(1)} %shard_map.91) | data formatting | bytes 262144
